TPU v7x, 256 devices: a whole 4x4x8 slice. The times are simulated.
256 devices in a mesh: ep: 64 (over z, x, core), tp: 4 (over y).
Axes of the slice: x: 4, y: 4, z: 8, core: 2. Of those that a mesh axis runs over, the one named last changes fastest.
Arguments:
- queries: bfloat16 [16384, 1024], P('ep', 'tp'), may hold values from -256 to 256
- key_rows: bfloat16 [16384, 1024], P('ep', 'tp'), may hold values from -8 to 8
- value_rows: bfloat16 [16384, 1024], P('ep', 'tp'), may hold values from -6 to 6
- head_lambda: float32 [8], P('tp'), may hold values from 0.3 to 0.8
- sub_gain: float32 [128], replicated, may hold values from 0.1 to 1.9
- out_weight: bfloat16 [1024, 2048], P('tp'), may hold values from -0.1875 to 0.1875
- expert_input: bfloat16 [12288, 2048], P('ep'), may hold values from -6 to 6
- norm_gain: float32 [2048], replicated, may hold values from 0.1 to 1.9
- route_ids: int32 [12288, 2], P('ep'), may hold values from 0 to 63, all different within a row; in each aligned block of 192 rows (0 to 191, 192 to 383, ...) at most 10 rows name the same one
- route_weight: float32 [12288, 2], P('ep'), may hold values from 0.25 to 1
- gate_weight: bfloat16 [64, 2048, 3584], P('ep', None, 'tp'), may hold values from -0.125 to 0.125
- up_weight: bfloat16 [64, 2048, 3584], P('ep', None, 'tp'), may hold values from -0.125 to 0.125
- down_weight: bfloat16 [64, 3584, 2048], P('ep', 'tp'), may hold values from -0.09375 to 0.09375
Outputs:
- mixer_out: bfloat16 [16384, 2048], P(('ep', 'tp'))
- expert_out: bfloat16 [12288, 2048], P('ep', 'tp')
Inputs may be any that keep to these rules, and one draw needn't show every extreme that they name: `route_ids`: each row names 2 different experts. In each aligned block of 192 rows no expert is named by more than 10 rows, a bound that some block reaches.
All inputs are finite; a program needn't handle non-finite values.
Results may differ from a plain program's by a relative error of at most 0.014.
Values may be sent and summed in bfloat16 or wider, within the bound.
A program may use at most 256 MiB of HBM per device.

v0:
```python
import jax
import jax.numpy as jnp
from jax import lax
from jax.sharding import PartitionSpec as P

EPS = 1e-06


def joined_along(parts, dim):
    lengths = list(parts.shape[1:])
    lengths[dim] *= parts.shape[0]
    return jnp.moveaxis(parts, 0, dim).reshape(lengths)


def copy_for_each(array, axis):
    devices = lax.axis_size(axis)
    return lax.all_to_all(
        jnp.broadcast_to(array[None], (devices, *array.shape)), axis, 0, 0, tiled=True
    )


def collect(array, axis, dim):
    return joined_along(copy_for_each(array, axis), dim)


def mixer_half(queries, key_rows, value_rows, head_lambda, sub_gain, out_weight):
    rows_here = queries.shape[0]
    heads_here = head_lambda.shape[0]
    head_width = queries.shape[1] // (2 * heads_here)
    value_width = value_rows.shape[1] // heads_here
    scaling = head_width ** (-0.5)
    query_blocks = queries.reshape(rows_here, heads_here, 2, head_width)
    query_pos = lax.axis_index("ep") * rows_here + jnp.arange(rows_here, dtype=jnp.int32)
    row_max = jnp.full((heads_here, 2, rows_here), -1e30, jnp.float32)
    key_piece = lax.all_gather(key_rows, "ep", axis=0, tiled=True)
    value_piece = lax.all_gather(value_rows, "ep", axis=0, tiled=True)
    length = key_piece.shape[0]
    key_blocks = key_piece.reshape(length, heads_here, 2, head_width)
    value_blocks = value_piece.reshape(length, heads_here, value_width)
    scores = (
        jnp.einsum("qhmd,khmd->hmqk", query_blocks, key_blocks, preferred_element_type=jnp.float32)
        * scaling
    )
    allowed = query_pos[:, None] >= jnp.arange(length, dtype=jnp.int32)[None, :]
    scores = jnp.where(allowed, scores, -1e30)
    new_max = jnp.maximum(row_max, jnp.max(scores, axis=-1))
    weights = jnp.where(allowed, jnp.exp(scores - new_max[..., None]), 0.0)
    row_total = jnp.sum(weights, axis=-1)
    numerator = jnp.einsum(
        "hmqk,khd->hmqd",
        weights.astype(jnp.bfloat16),
        value_blocks,
        preferred_element_type=jnp.float32,
    )
    row_max, row_total, numerator = (new_max, row_total, numerator)
    per_map = numerator / row_total[..., None]
    contrast = per_map[:, 0] - head_lambda[:, None, None] * per_map[:, 1]
    normed = (
        contrast * lax.rsqrt(jnp.mean(contrast * contrast, axis=-1, keepdims=True) + EPS) * sub_gain
    ).astype(jnp.bfloat16)
    attended = jnp.transpose(normed, (1, 0, 2)).reshape(rows_here, heads_here * value_width)
    return lax.psum_scatter(
        jnp.dot(attended, out_weight, preferred_element_type=jnp.float32).astype(jnp.bfloat16),
        "tp",
        scatter_dimension=0,
        tiled=True,
    )


def expert_half(
    expert_input, norm_gain, route_ids, route_weight, gate_weight, up_weight, down_weight
):
    rows_here, model_width = expert_input.shape
    experts = lax.axis_size("ep")
    top_count = route_ids.shape[1]
    capacity = 5 * top_count * rows_here // (3 * experts)
    slots = experts * capacity
    wide_rows = expert_input.astype(jnp.float32)
    normed = (
        wide_rows
        * lax.rsqrt(jnp.mean(wide_rows * wide_rows, axis=-1, keepdims=True) + EPS)
        * norm_gain
    ).astype(jnp.bfloat16)
    flat_ids = route_ids.reshape(-1)
    onehot = (flat_ids[:, None] == jnp.arange(experts, dtype=jnp.int32)[None, :]).astype(jnp.int32)
    rank_before = jnp.cumsum(onehot, axis=0) - onehot
    slot_index = jnp.sum(rank_before * onehot, axis=1)
    buffer_pos = (flat_ids * capacity + slot_index).reshape(rows_here, top_count)
    matches = buffer_pos[None, :, :] == jnp.arange(slots, dtype=jnp.int32)[:, None, None]
    dispatch = jnp.any(matches, axis=-1).astype(jnp.bfloat16)
    combine = jnp.sum(jnp.where(matches, route_weight[None, :, :], 0.0), axis=-1)
    gate_mat = gate_weight[0]
    up_mat = up_weight[0]
    down_mat = down_weight[0]
    column_share = model_width // lax.axis_size("tp")
    own_cols = lax.dynamic_slice_in_dim(
        normed, lax.axis_index("tp") * column_share, column_share, 1
    )
    outgoing = jnp.dot(dispatch, own_cols, preferred_element_type=jnp.float32).astype(jnp.bfloat16)
    arrived = lax.all_to_all(
        outgoing.reshape(experts, capacity, column_share),
        "ep",
        split_axis=0,
        concat_axis=0,
        tiled=True,
    ).reshape(slots, column_share)
    pieces = collect(arrived, "tp", 1)
    gate_act = jnp.dot(pieces, gate_mat, preferred_element_type=jnp.float32)
    up_act = jnp.dot(pieces, up_mat, preferred_element_type=jnp.float32)
    hidden = (jax.nn.silu(gate_act) * up_act).astype(jnp.bfloat16)
    partial_result = jnp.dot(hidden, down_mat, preferred_element_type=jnp.float32)
    summed = lax.psum_scatter(
        partial_result.astype(jnp.bfloat16), "tp", scatter_dimension=1, tiled=True
    )
    col_count = summed.shape[1]
    returned = lax.all_to_all(
        summed.reshape(experts, capacity, col_count), "ep", split_axis=0, concat_axis=0, tiled=True
    ).reshape(slots, col_count)
    mixed = lax.dot_general(
        combine,
        returned.astype(jnp.float32),
        (((0,), (0,)), ((), ())),
        preferred_element_type=jnp.float32,
    )
    return mixed.astype(jnp.bfloat16)


def shards(
    queries,
    key_rows,
    value_rows,
    head_lambda,
    sub_gain,
    out_weight,
    expert_input,
    norm_gain,
    route_ids,
    route_weight,
    gate_weight,
    up_weight,
    down_weight,
):
    mixer_out = mixer_half(queries, key_rows, value_rows, head_lambda, sub_gain, out_weight)
    expert_out = expert_half(
        expert_input, norm_gain, route_ids, route_weight, gate_weight, up_weight, down_weight
    )
    return (mixer_out, expert_out)


def solution(mesh):
    placed = (
        P("ep", "tp"),
        P("ep", "tp"),
        P("ep", "tp"),
        P("tp"),
        P(),
        P("tp", None),
        P("ep", None),
        P(),
        P("ep", None),
        P("ep", None),
        P("ep", None, "tp"),
        P("ep", None, "tp"),
        P("ep", "tp", None),
    )
    return jax.shard_map(
        shards,
        mesh=mesh,
        in_specs=placed,
        out_specs=(P(("ep", "tp"), None), P("ep", "tp")),
        check_vma=False,
    )
```

profile of v0, /device:TPU:1, one launch (start us, length us, event | category | flops | bytes accessed | tf_op | source)
XLA Modules:
  0.0 275.6 jit_solution(8443543517170979029)
XLA Ops:
  8.0 0.0 all-gather.3.cloned.1.call-start
  8.1 0.7 all-gather.3.cloned.1.call-update
  8.8 0.0 all-gather.5.cloned.1.call-start
  8.8 0.7 all-gather.5.cloned.1.call-update
  9.5 0.8 copy.47
  10.3 0.1 eq.38
  10.5 0.1 eq.42
  10.6 0.9 reduce-window.6
  11.5 0.2 slice_reduce_fusion
  11.8 0.1 fusion.32
  11.9 0.1 reduce_sum.50
  12.1 0.1 copy.50
  12.1 1.3 convert_element_type.41
  13.5 0.8 dynamic-slice
  14.2 0.7 multiply_add_fusion
  14.9 0.1 fusion.20
  15.1 0.2 multiply_reduce_fusion
  15.3 0.5 convolution_convert_fusion.1
  15.8 1.3 reshape.86
  17.1 13.0 %all-to-all-start = ((bf16[64,10,512]{2,1,0:T(8,128)(2,1)}), bf16[64,10,512]{2,1,0:T(8,128)(2,1)S(1)}, u32[]{:S(2)}, u32[]{:S(2)}) async-start(bf16[64,10,512]{2,1,0:T(8,128)(2,1)} %reshape.86), calls=%async_computation.1 | async-start | bytes 2097152 | tf_op jit(solution)/shard_map/all_to_all | solution.py:100
  30.1 0.1 copy.43
  30.2 32.2 %all-to-all-done = bf16[64,10,512]{2,1,0:T(8,128)(2,1)S(1)} async-done(((bf16[64,10,512]{2,1,0:T(8,128)(2,1)}), bf16[64,10,512]{2,1,0:T(8,128)(2,1)S(1)}, u32[]{:S(2)}, u32[]{:S(2)}) %all-to-all-start) | async-done | bytes 655392 | tf_op jit(solution)/shard_map/all_to_all | solution.py:100
  62.4 0.2 broadcast_in_dim.52
  62.7 0.3 copy.51
  63.0 1.9 broadcast_in_dim.53
  64.8 4.6 %all-to-all-start.1 = ((bf16[4,640,512]{1,2,0:T(8,128)(2,1)}), bf16[4,640,512]{1,2,0:T(8,128)(2,1)}, u32[]{:S(2)}, u32[]{:S(2)}) async-start(bf16[4,640,512]{1,2,0:T(8,128)(2,1)} %broadcast_in_dim.53), calls=%async_computation.2 | async-start | bytes 5242880 | tf_op jit(solution)/shard_map/all_to_all | solution.py:17
  69.4 0.2 reduce-scatter.5.cloned.1.call-start
  69.6 4.5 %iota_compare_fusion = pred[256,16384]{1,0:T(8,128)(4,1)} fusion(s32[256]{0:T(256)S(1)} %iota_add_fusion), kind=kLoop, calls=%fused_computation.7 | loop fusion | flops 4194304 | bytes 4195328 | tf_op jit(solution)/shard_map/ge | solution.py:44
  74.1 26.2 %all-to-all-done.1 = bf16[4,640,512]{1,2,0:T(8,128)(2,1)} async-done(((bf16[4,640,512]{1,2,0:T(8,128)(2,1)}), bf16[4,640,512]{1,2,0:T(8,128)(2,1)}, u32[]{:S(2)}, u32[]{:S(2)}) %all-to-all-start.1) | async-done | bytes 2621472 | tf_op jit(solution)/shard_map/all_to_all | solution.py:17
  100.4 7.2 %fusion.10 = f32[640,896]{1,0:T(8,128)} fusion(bf16[640,2048]{0,1:T(8,128)(2,1)} %bitcast.11, bf16[1,2048,896]{2,1,0:T(8,128)(2,1)} %param.23), kind=kOutput, calls=%fused_computation.12 | convolution fusion | flops 2348810240 | bytes 8585216 | tf_op jit(solution)/shard_map/dot_general | solution.py:108
  107.6 11.9 %fusion.12 = bf16[640,2048]{1,0:T(8,128)(2,1)} fusion(bf16[1,896,2048]{2,1,0:T(8,128)(2,1)} %param.25, f32[640,896]{1,0:T(8,128)} %fusion.10, bf16[640,2048]{0,1:T(8,128)(2,1)} %bitcast.11, bf16[1,2048,896]{2,1,0:T(8,128)(2,1)} %param.24), kind=kOutput, calls=%fused_computation.14 | convolution fusion | flops 4702371840 | bytes 14876672 | tf_op jit(solution)/shard_map/dot_general | solution.py:111
  119.5 0.3 reduce-scatter.3.cloned.1.call-start
  119.8 0.0 all-gather.3.cloned.1.call-done
  119.8 12.0 %copy.44 = bf16[16384,256]{0,1:T(8,128)(2,1)} copy(bf16[16384,256]{1,0:T(8,128)(2,1)} %all-gather.3.cloned.1.call-done) | data formatting | bytes 16777216 | tf_op jit(solution)/shard_map/all_gather | solution.py:35
  131.8 31.4 %fusion = (f32[2,2,256]{2,1,0:T(2,128)S(1)}, f32[2,2,256,16384]{3,2,1,0:T(8,128)}) fusion(pred[256,16384]{1,0:T(8,128)(4,1)} %iota_compare_fusion, bf16[256,2,2,64]{0,3,2,1:T(8,128)(2,1)S(1)} %bitcast.81, bf16[16384,2,2,64]{0,3,2,1:T(8,128)(2,1)} %bitcast.79), kind=kOutput, calls=%fused_computation.2 | convolution fusion | flops 2197814272 | bytes 79826944 | tf_op jit(solution)/shard_map/qhmd,khmd->hmqk/dot_general | solution.py:41
  163.2 24.2 %fusion.1 = f32[2,2,256]{2,1,0:T(2,128)S(1)} fusion(f32[2,2,256,16384]{3,2,1,0:T(8,128)} %get-tuple-element.3, f32[2,2,256]{2,1,0:T(2,128)S(1)} %broadcast_maximum_fusion, pred[256,16384]{1,0:T(8,128)(4,1)} %iota_compare_fusion), kind=kLoop, calls=%fused_computation.3 | loop fusion | flops 83885056 | bytes 71311360 | tf_op jit(solution)/shard_map/reduce_sum | solution.py:48
  187.4 12.0 %copy.45 = bf16[16384,256]{0,1:T(8,128)(2,1)} copy(bf16[16384,256]{1,0:T(8,128)(2,1)} %all-gather.5.cloned.1.call-done) | data formatting | bytes 16777216 | tf_op jit(solution)/shard_map/all_gather | solution.py:36
  199.4 28.4 %fusion.17 = f32[2,2,256,128]{2,3,1,0:T(8,128)S(1)} fusion(bf16[16384,2,128,1]{0,2,3,1:T(8,128)(2,1)} %bitcast.78, f32[2,2,256,16384]{3,2,1,0:T(8,128)} %get-tuple-element.3, f32[2,2,256]{2,1,0:T(2,128)S(1)} %broadcast_maximum_fusion, pred[256,16384]{1,0:T(8,128)(4,1)} %iota_compare_fusion, f32[2,2,256]{2,1,0:T(2,128)S(1)} %fusion.1), kind=kOutput, calls=%fused_computation.19 | convolution fusion | flops 4378984448 | bytes 80224256 | tf_op jit(solution)/shard_map/hmqk,khd->hmqd/dot_general | solution.py:49
  227.8 0.1 multiply_reduce_fusion.1
  227.9 0.1 multiply_convert_fusion.1
  228.1 1.5 convolution_convert_fusion
  229.5 0.0 reduce-scatter.5.cloned.1.call-done
  229.6 2.2 reshape.88
  231.8 7.0 %all-to-all-start.2 = ((bf16[64,10,512]{2,1,0:T(8,128)(2,1)}), bf16[64,10,512]{2,1,0:T(8,128)(2,1)S(1)}, u32[]{:S(2)}, u32[]{:S(2)}) async-start(bf16[64,10,512]{2,1,0:T(8,128)(2,1)} %reshape.88), calls=%async_computation.4 | async-start | bytes 2097152 | tf_op jit(solution)/shard_map/all_to_all | solution.py:116
  238.8 0.2 select_reduce_fusion
  239.0 28.0 %all-to-all-done.2 = bf16[64,10,512]{2,1,0:T(8,128)(2,1)S(1)} async-done(((bf16[64,10,512]{2,1,0:T(8,128)(2,1)}), bf16[64,10,512]{2,1,0:T(8,128)(2,1)S(1)}, u32[]{:S(2)}, u32[]{:S(2)}) %all-to-all-start.2) | async-done | bytes 655392 | tf_op jit(solution)/shard_map/all_to_all | solution.py:116
  266.9 0.2 reshape.89
  267.2 1.0 fusion.39
  (22 shorter events, 0.2 us)
Async XLA Ops:
  8.0 220.1 %copy-start = (bf16[256,2048]{1,0:T(8,128)(2,1)S(1)}, bf16[256,2048]{1,0:T(8,128)(2,1)}, u32[]{:S(2)}) copy-start(bf16[256,2048]{1,0:T(8,128)(2,1)} %param.18) | copy-start | bytes 3145732
  8.0 7.1 %copy-start.1 = (bf16[192,2048]{1,0:T(8,128)(2,1)S(1)}, bf16[192,2048]{1,0:T(8,128)(2,1)}, u32[]{:S(2)}) copy-start(bf16[192,2048]{1,0:T(8,128)(2,1)} %param.19) | copy-start | bytes 2359300
  8.0 111.8 %all-gather.3.cloned.1.call-start = ((), (), s32[]{:S(2)}) async-start(), calls=%async_computation.5 | async-start | bytes 8519680 | tf_op jit(solution)/shard_map/all_gather | solution.py:35
  8.8 178.6 %all-gather.5.cloned.1.call-start = ((), (), s32[]{:S(2)}) async-start(), calls=%async_computation.6 | async-start | bytes 8519680 | tf_op jit(solution)/shard_map/all_gather | solution.py:36
  12.1 18.0 %copy-start.2 = (bf16[256,256]{1,0:T(8,128)(2,1)S(1)}, bf16[256,256]{1,0:T(8,128)(2,1)}, u32[]{:S(2)}) copy-start(bf16[256,256]{1,0:T(8,128)(2,1)} %param.13) | copy-start | bytes 393220
  17.1 45.4 %all-to-all-start = ((bf16[64,10,512]{2,1,0:T(8,128)(2,1)}), bf16[64,10,512]{2,1,0:T(8,128)(2,1)S(1)}, u32[]{:S(2)}, u32[]{:S(2)}) async-start(bf16[64,10,512]{2,1,0:T(8,128)(2,1)} %reshape.86), calls=%async_computation.1 | async-start | bytes 2097152 | tf_op jit(solution)/shard_map/all_to_all | solution.py:100
  64.8 35.5 %all-to-all-start.1 = ((bf16[4,640,512]{1,2,0:T(8,128)(2,1)}), bf16[4,640,512]{1,2,0:T(8,128)(2,1)}, u32[]{:S(2)}, u32[]{:S(2)}) async-start(bf16[4,640,512]{1,2,0:T(8,128)(2,1)} %broadcast_in_dim.53), calls=%async_computation.2 | async-start | bytes 5242880 | tf_op jit(solution)/shard_map/all_to_all | solution.py:17
  69.4 160.1 %reduce-scatter.5.cloned.1.call-start = ((), (), s32[]{:S(2)}) async-start(), calls=%async_computation.8 | async-start | bytes 3276800 | tf_op jit(solution)/shard_map/reduce_scatter | solution.py:112
  119.5 148.7 %reduce-scatter.3.cloned.1.call-start = ((), (), s32[]{:S(2)}) async-start(), calls=%async_computation.7 | async-start | bytes 1310720 | tf_op jit(solution)/shard_map/reduce_scatter | solution.py:62
  199.3 28.4 %copy-start.4 = (f32[2]{0:T(128)S(1)}, f32[2]{0:T(128)}, u32[]{:S(2)}) copy-start(f32[2]{0:T(128)} %param.16) | copy-start | bytes 28
  199.3 28.6 %copy-start.5 = (f32[128]{0:T(128)S(1)}, f32[128]{0:T(128)}, u32[]{:S(2)}) copy-start(f32[128]{0:T(128)} %param.17) | copy-start | bytes 1540
  227.8 11.0 %copy-start.3 = (f32[192,2]{0,1:T(2,128)S(1)}, f32[192,2]{0,1:T(2,128)}, u32[]{:S(2)}) copy-start(f32[192,2]{0,1:T(2,128)} %param.22) | copy-start | bytes 4612
  231.8 35.2 %all-to-all-start.2 = ((bf16[64,10,512]{2,1,0:T(8,128)(2,1)}), bf16[64,10,512]{2,1,0:T(8,128)(2,1)S(1)}, u32[]{:S(2)}, u32[]{:S(2)}) async-start(bf16[64,10,512]{2,1,0:T(8,128)(2,1)} %reshape.88), calls=%async_computation.4 | async-start | bytes 2097152 | tf_op jit(solution)/shard_map/all_to_all | solution.py:116
Sparse Core Ops, SparseCore 0:
  11.6 90.9 all-gather.2
  105.3 79.7 all-gather.4
Sparse Core Ops, SparseCore 1:
  119.6 32.6 reduce-scatter.4
  229.6 20.7 reduce-scatter.2
where the time goes:
time: 277 us; the launch traced here: 276 us
  waiting for transfers between devices  87.9 us (32%)
  matrix products  81.8 us (30%)
  other arithmetic  32.6 us (12%)
  local copies, waits for them, and re-layouts  32.5 us (12%)
  starting transfers between devices  25.1 us (9%)
  between operations  15.8 us (6%)
    all_to_all x1, waiting for transfers between devices, expert_half(): lax.all_to_all(outgoing.reshape(experts, capacity, column_share), 'ep', s...  32.2 us
    dot_general x1, matrix products, mixer_half(): jnp.einsum('qhmd,khmd->hmqk', query_blocks, key_blocks, preferred_element...  31.4 us
    dot_general x1, matrix products, mixer_half(): jnp.einsum('hmqk,khd->hmqd', weights.astype(jnp.bfloat16), value_blocks,...  28.4 us
    all_to_all x1, waiting for transfers between devices, expert_half(): lax.all_to_all(summed.reshape(experts, capacity, col_count), 'ep', split_...  28 us
    all_to_all x1, waiting for transfers between devices, copy_for_each(): lax.all_to_all(jnp.broadcast_to(array[None], (devices, *array.shape)), ax...  26.2 us
    reduce_sum x1, other arithmetic, mixer_half(): row_total = jnp.sum(weights, axis=-1)  24.2 us
    all_to_all x1, starting transfers between devices, expert_half(): lax.all_to_all(outgoing.reshape(experts, capacity, column_share), 'ep', s...  13 us
    all_gather x1, local copies, waits for them, and re-layouts, mixer_half(): key_piece = lax.all_gather(key_rows, 'ep', axis=0, tiled=True)  12 us
  transfers between devices with their start and end apart: 7, of which 3 were waited for; matrix products, arithmetic and copies ran while one was open for 53% of the time, Pallas kernels for 0%

commit v1 on v0

--- a/solution.py
+++ b/solution.py
@@ -32,8 +32,11 @@
     query_blocks = queries.reshape(rows_here, heads_here, 2, head_width)
     query_pos = lax.axis_index("ep") * rows_here + jnp.arange(rows_here, dtype=jnp.int32)
     row_max = jnp.full((heads_here, 2, rows_here), -1e30, jnp.float32)
-    key_piece = lax.all_gather(key_rows, "ep", axis=0, tiled=True)
-    value_piece = lax.all_gather(value_rows, "ep", axis=0, tiled=True)
+    key_piece, value_piece = jnp.split(
+        lax.all_gather(jnp.concatenate([key_rows, value_rows], axis=1), "ep", axis=0, tiled=True),
+        [key_rows.shape[1]],
+        axis=1,
+    )
     length = key_piece.shape[0]
     key_blocks = key_piece.reshape(length, heads_here, 2, head_width)
     value_blocks = value_piece.reshape(length, heads_here, value_width)

time: 277 us -> 289 us (1.043)
  local copies, waits for them, and re-layouts: 32.5 us -> 44.3 us
  waiting for transfers between devices: 87.9 us -> 91.9 us
  matrix products: 81.8 us -> 78.5 us
    split x0 -> x3, local copies, waits for them, and re-layouts: none -> 35.4 us  [mixer_half(): jnp.split(lax.all_gather(jnp.concatenate([key_rows, value_rows], axis=1),...]
    all_gather x2 -> x0, local copies, waits for them, and re-layouts: 24 us -> none  [the longest x1 12 us: mixer_half(): key_piece = lax.all_gather(key_rows, 'ep', axis=0, tiled=True)]
    all_to_all x1, waiting for transfers between devices: 32.2 us -> 36.7 us  [expert_half(): lax.all_to_all(outgoing.reshape(experts, capacity, column_share), 'ep', s...]
    dot_general x1, matrix products: 31.4 us -> 27.8 us  [mixer_half(): jnp.einsum('qhmd,khmd->hmqk', query_blocks, key_blocks, preferred_element...]
  transfers between devices with their start and end apart: 7 -> 6, of which waited for: 3 -> 3; matrix products, arithmetic and copies ran while one was open for 53% -> 53% of each run, Pallas kernels for 0% -> 0%
where the time goes in v1:
time: 289 us; the launch traced here: 288 us
  waiting for transfers between devices  91.9 us (32%)
  matrix products  78.5 us (27%)
  local copies, waits for them, and re-layouts  44.3 us (15%)
  other arithmetic  32.7 us (11%)
  starting transfers between devices  24.4 us (8%)
  between operations  15.8 us (5%)
    all_to_all x1, waiting for transfers between devices, expert_half(): lax.all_to_all(outgoing.reshape(experts, capacity, column_share), 'ep', s...  36.7 us
    split x3, local copies, waits for them, and re-layouts, mixer_half(): jnp.split(lax.all_gather(jnp.concatenate([key_rows, value_rows], axis=1),...  35.4 us
    dot_general x1, matrix products, mixer_half(): jnp.einsum('hmqk,khd->hmqd', weights.astype(jnp.bfloat16), value_blocks,...  28.3 us
    all_to_all x1, waiting for transfers between devices, expert_half(): lax.all_to_all(summed.reshape(experts, capacity, col_count), 'ep', split_...  28 us
    dot_general x1, matrix products, mixer_half(): jnp.einsum('qhmd,khmd->hmqk', query_blocks, key_blocks, preferred_element...  27.8 us
    all_to_all x1, waiting for transfers between devices, copy_for_each(): lax.all_to_all(jnp.broadcast_to(array[None], (devices, *array.shape)), ax...  27.2 us
    reduce_sum x1, other arithmetic, mixer_half(): row_total = jnp.sum(weights, axis=-1)  22.9 us
    all_to_all x1, starting transfers between devices, expert_half(): lax.all_to_all(outgoing.reshape(experts, capacity, column_share), 'ep', s...  13 us
  transfers between devices with their start and end apart: 6, of which 3 were waited for; matrix products, arithmetic and copies ran while one was open for 53% of the time, Pallas kernels for 0%

profile of v1, /device:TPU:1, one launch (start us, length us, event | category | flops | bytes accessed | tf_op | source)
XLA Modules:
  0.0 287.6 jit_solution(12097962733637082015)
XLA Ops:
  8.0 0.0 all-gather.2.cloned.1.call-start
  8.1 1.8 pad_maximum_fusion
  9.9 0.8 copy.51
  10.7 0.1 eq.38
  10.9 0.1 eq.42
  11.0 0.9 reduce-window.6
  11.9 0.2 slice_reduce_fusion
  12.2 0.1 fusion.32
  12.3 0.1 reduce_sum.50
  12.5 0.1 copy.54
  12.5 1.3 convert_element_type.41
  13.9 0.8 dynamic-slice
  14.6 0.7 multiply_add_fusion
  15.3 0.6 copy-done.3
  15.9 0.1 fusion.17
  16.1 0.2 multiply_reduce_fusion
  16.3 0.5 convolution_convert_fusion.1
  16.8 1.2 reshape.86
  18.0 13.0 %all-to-all-start = ((bf16[64,10,512]{2,1,0:T(8,128)(2,1)}), bf16[64,10,512]{2,1,0:T(8,128)(2,1)S(1)}, u32[]{:S(2)}, u32[]{:S(2)}) async-start(bf16[64,10,512]{2,1,0:T(8,128)(2,1)} %reshape.86), calls=%async_computation.1 | async-start | bytes 2097152 | tf_op jit(solution)/shard_map/all_to_all | solution.py:103
  31.0 0.1 copy.47
  31.1 36.7 %all-to-all-done = bf16[64,10,512]{2,1,0:T(8,128)(2,1)S(1)} async-done(((bf16[64,10,512]{2,1,0:T(8,128)(2,1)}), bf16[64,10,512]{2,1,0:T(8,128)(2,1)S(1)}, u32[]{:S(2)}, u32[]{:S(2)}) %all-to-all-start) | async-done | bytes 655392 | tf_op jit(solution)/shard_map/all_to_all | solution.py:103
  67.8 0.2 broadcast_in_dim.52
  68.0 0.3 copy.55
  68.3 1.7 broadcast_in_dim.53
  70.0 4.6 %all-to-all-start.1 = ((bf16[4,640,512]{1,2,0:T(8,128)(2,1)}), bf16[4,640,512]{1,2,0:T(8,128)(2,1)}, u32[]{:S(2)}, u32[]{:S(2)}) async-start(bf16[4,640,512]{1,2,0:T(8,128)(2,1)} %broadcast_in_dim.53), calls=%async_computation.2 | async-start | bytes 5242880 | tf_op jit(solution)/shard_map/all_to_all | solution.py:17
  74.6 0.0 reduce-scatter.5.cloned.1.call-start
  74.6 4.1 %iota_compare_fusion = pred[256,16384]{0,1:T(8,128)(4,1)} fusion(s32[256]{0:T(256)S(1)} %iota_add_fusion), kind=kLoop, calls=%fused_computation.7 | loop fusion | flops 4194304 | bytes 4195328 | tf_op jit(solution)/shard_map/ge | solution.py:47
  78.8 27.2 %all-to-all-done.1 = bf16[4,640,512]{1,2,0:T(8,128)(2,1)} async-done(((bf16[4,640,512]{1,2,0:T(8,128)(2,1)}), bf16[4,640,512]{1,2,0:T(8,128)(2,1)}, u32[]{:S(2)}, u32[]{:S(2)}) %all-to-all-start.1) | async-done | bytes 2621472 | tf_op jit(solution)/shard_map/all_to_all | solution.py:17
  105.9 7.3 %fusion.10 = f32[640,896]{1,0:T(8,128)} fusion(bf16[640,2048]{0,1:T(8,128)(2,1)} %bitcast.12, bf16[1,2048,896]{2,1,0:T(8,128)(2,1)} %param.23), kind=kOutput, calls=%fused_computation.12 | convolution fusion | flops 2348810240 | bytes 8585216 | tf_op jit(solution)/shard_map/dot_general | solution.py:111
  113.2 12.2 %fusion.12 = bf16[640,2048]{1,0:T(8,128)(2,1)} fusion(bf16[1,896,2048]{2,1,0:T(8,128)(2,1)} %param.25, f32[640,896]{1,0:T(8,128)} %fusion.10, bf16[640,2048]{0,1:T(8,128)(2,1)} %bitcast.12, bf16[1,2048,896]{2,1,0:T(8,128)(2,1)} %param.24), kind=kOutput, calls=%fused_computation.14 | convolution fusion | flops 4702371840 | bytes 14876672 | tf_op jit(solution)/shard_map/dot_general | solution.py:114
  125.4 0.2 reduce-scatter.3.cloned.1.call-start
  125.6 0.0 all-gather.2.cloned.1.call-done
  125.7 11.4 %fusion.39 = (bf16[16384,256]{1,0:T(8,128)(2,1)}, bf16[16384,256]{1,0:T(8,128)(2,1)}) fusion(bf16[16384,512]{1,0:T(8,128)(2,1)} %all-gather.2.cloned.1.call-done), kind=kLoop, calls=%fused_computation.55 | loop fusion | bytes 33554432 | tf_op jit(solution)/shard_map/split | solution.py:35
  137.1 12.0 %copy.48 = bf16[16384,256]{0,1:T(8,128)(2,1)} copy(bf16[16384,256]{1,0:T(8,128)(2,1)} %get-tuple-element.3) | data formatting | bytes 16777216 | tf_op jit(solution)/shard_map/split | solution.py:35
  149.1 12.0 %copy.46 = bf16[16384,256]{0,1:T(8,128)(2,1)} copy(bf16[16384,256]{1,0:T(8,128)(2,1)} %get-tuple-element.2) | data formatting | bytes 16777216 | tf_op jit(solution)/shard_map/split | solution.py:35
  161.1 27.8 %fusion = (f32[2,2,256]{2,1,0:T(2,128)S(1)}, f32[2,2,16384,256]{3,2,1,0:T(8,128)}) fusion(pred[256,16384]{0,1:T(8,128)(4,1)} %iota_compare_fusion, bf16[16384,2,2,64]{0,3,2,1:T(8,128)(2,1)} %bitcast.92, bf16[256,2,2,64]{0,3,2,1:T(8,128)(2,1)S(1)} %bitcast.94), kind=kOutput, calls=%fused_computation.2 | convolution fusion | flops 2197814272 | bytes 79826944 | tf_op jit(solution)/shard_map/qhmd,khmd->hmqk/dot_general | solution.py:44
  188.9 22.9 %fusion.1 = f32[2,2,256]{2,1,0:T(2,128)S(1)} fusion(f32[2,2,16384,256]{3,2,1,0:T(8,128)} %get-tuple-element.5, f32[2,2,256]{2,1,0:T(2,128)S(1)} %broadcast_maximum_fusion, pred[256,16384]{0,1:T(8,128)(4,1)} %iota_compare_fusion), kind=kLoop, calls=%fused_computation.3 | loop fusion | flops 83885056 | bytes 71311360 | tf_op jit(solution)/shard_map/reduce_sum | solution.py:51
  211.8 28.3 %fusion.22 = f32[2,2,256,128]{2,3,1,0:T(8,128)S(1)} fusion(bf16[16384,2,128,1]{0,2,3,1:T(8,128)(2,1)} %bitcast.91, f32[2,2,16384,256]{3,2,1,0:T(8,128)} %get-tuple-element.5, f32[2,2,256]{2,1,0:T(2,128)S(1)} %broadcast_maximum_fusion, pred[256,16384]{0,1:T(8,128)(4,1)} %iota_compare_fusion, f32[2,2,256]{2,1,0:T(2,128)S(1)} %fusion.1), kind=kOutput, calls=%fused_computation.26 | convolution fusion | flops 4378984448 | bytes 80224256 | tf_op jit(solution)/shard_map/hmqk,khd->hmqd/dot_general | solution.py:52
  240.2 0.1 multiply_reduce_fusion.1
  240.3 0.1 multiply_convert_fusion.1
  240.4 1.5 convolution_convert_fusion
  241.9 0.0 reduce-scatter.5.cloned.1.call-done
  242.0 2.2 reshape.88
  244.1 6.6 %all-to-all-start.2 = ((bf16[64,10,512]{2,1,0:T(8,128)(2,1)}), bf16[64,10,512]{2,1,0:T(8,128)(2,1)S(1)}, u32[]{:S(2)}, u32[]{:S(2)}) async-start(bf16[64,10,512]{2,1,0:T(8,128)(2,1)} %reshape.88), calls=%async_computation.4 | async-start | bytes 2097152 | tf_op jit(solution)/shard_map/all_to_all | solution.py:119
  250.8 0.2 select_reduce_fusion
  251.0 28.0 %all-to-all-done.2 = bf16[64,10,512]{2,1,0:T(8,128)(2,1)S(1)} async-done(((bf16[64,10,512]{2,1,0:T(8,128)(2,1)}), bf16[64,10,512]{2,1,0:T(8,128)(2,1)S(1)}, u32[]{:S(2)}, u32[]{:S(2)}) %all-to-all-start.2) | async-done | bytes 655392 | tf_op jit(solution)/shard_map/all_to_all | solution.py:119
  278.9 0.2 reshape.89
  279.1 1.0 fusion.40
  (25 shorter events, 0.2 us)
Async XLA Ops:
  8.0 232.4 %copy-start = (bf16[256,2048]{1,0:T(8,128)(2,1)S(1)}, bf16[256,2048]{1,0:T(8,128)(2,1)}, u32[]{:S(2)}) copy-start(bf16[256,2048]{1,0:T(8,128)(2,1)} %param.18) | copy-start | bytes 3145732
  8.0 8.0 %copy-start.1 = (bf16[192,2048]{1,0:T(8,128)(2,1)S(1)}, bf16[192,2048]{1,0:T(8,128)(2,1)}, u32[]{:S(2)}) copy-start(bf16[192,2048]{1,0:T(8,128)(2,1)} %param.19) | copy-start | bytes 2359300
  8.0 117.6 %all-gather.2.cloned.1.call-start = ((), (), s32[]{:S(2)}) async-start(), calls=%async_computation.5 | async-start | bytes 17039360 | tf_op jit(solution)/shard_map/all_gather | solution.py:36
  12.5 18.5 %copy-start.2 = (bf16[256,256]{1,0:T(8,128)(2,1)S(1)}, bf16[256,256]{1,0:T(8,128)(2,1)}, u32[]{:S(2)}) copy-start(bf16[256,256]{1,0:T(8,128)(2,1)} %param.13) | copy-start | bytes 393220
  15.3 0.6 copy-start.3
  18.0 49.8 %all-to-all-start = ((bf16[64,10,512]{2,1,0:T(8,128)(2,1)}), bf16[64,10,512]{2,1,0:T(8,128)(2,1)S(1)}, u32[]{:S(2)}, u32[]{:S(2)}) async-start(bf16[64,10,512]{2,1,0:T(8,128)(2,1)} %reshape.86), calls=%async_computation.1 | async-start | bytes 2097152 | tf_op jit(solution)/shard_map/all_to_all | solution.py:103
  70.0 35.9 %all-to-all-start.1 = ((bf16[4,640,512]{1,2,0:T(8,128)(2,1)}), bf16[4,640,512]{1,2,0:T(8,128)(2,1)}, u32[]{:S(2)}, u32[]{:S(2)}) async-start(bf16[4,640,512]{1,2,0:T(8,128)(2,1)} %broadcast_in_dim.53), calls=%async_computation.2 | async-start | bytes 5242880 | tf_op jit(solution)/shard_map/all_to_all | solution.py:17
  74.6 167.4 %reduce-scatter.5.cloned.1.call-start = ((), (), s32[]{:S(2)}) async-start(), calls=%async_computation.7 | async-start | bytes 3276800 | tf_op jit(solution)/shard_map/reduce_scatter | solution.py:115
  125.4 154.8 %reduce-scatter.3.cloned.1.call-start = ((), (), s32[]{:S(2)}) async-start(), calls=%async_computation.6 | async-start | bytes 1310720 | tf_op jit(solution)/shard_map/reduce_scatter | solution.py:65
  211.8 28.4 %copy-start.6 = (f32[2]{0:T(128)S(1)}, f32[2]{0:T(128)}, u32[]{:S(2)}) copy-start(f32[2]{0:T(128)} %param.16) | copy-start | bytes 28
  211.8 28.5 %copy-start.7 = (f32[128]{0:T(128)S(1)}, f32[128]{0:T(128)}, u32[]{:S(2)}) copy-start(f32[128]{0:T(128)} %param.17) | copy-start | bytes 1540
  240.2 10.6 %copy-start.4 = (s32[192,2]{0,1:T(2,128)S(1)}, s32[192,2]{0,1:T(2,128)}, u32[]{:S(2)}) copy-start(s32[192,2]{0,1:T(2,128)} %copy-done.3) | copy-start | bytes 4612
  240.2 10.6 %copy-start.5 = (f32[192,2]{0,1:T(2,128)S(1)}, f32[192,2]{0,1:T(2,128)}, u32[]{:S(2)}) copy-start(f32[192,2]{0,1:T(2,128)} %param.22) | copy-start | bytes 4612
  244.1 34.8 %all-to-all-start.2 = ((bf16[64,10,512]{2,1,0:T(8,128)(2,1)}), bf16[64,10,512]{2,1,0:T(8,128)(2,1)S(1)}, u32[]{:S(2)}, u32[]{:S(2)}) async-start(bf16[64,10,512]{2,1,0:T(8,128)(2,1)} %reshape.88), calls=%async_computation.4 | async-start | bytes 2097152 | tf_op jit(solution)/shard_map/all_to_all | solution.py:119
Sparse Core Ops, SparseCore 0:
  12.2 112.6 all-gather.1
Sparse Core Ops, SparseCore 1:
  125.5 32.1 reduce-scatter.4
  242.0 20.7 reduce-scatter.2
